TPU v7x, 512 devices: a whole 4x8x8 slice. The times are simulated.
512 devices in a mesh: ep: 32 (over z, x), tp: 16 (over y, core).
Axes of the slice: x: 4, y: 8, z: 8, core: 2. Of those that a mesh axis runs over, the one named last changes fastest.
Arguments:
- tokens: bfloat16 [131072, 2048], P(('ep', 'tp')), may hold values from -6 to 6
- pre_gain: float32 [2048], replicated, may hold values from 0.1 to 1.9
- post_gain: float32 [2048], replicated, may hold values from 0.1 to 1.9
- expert_ids: int32 [131072, 2], P(('ep', 'tp')), may hold values from 0 to 31, as said below
- route_weight: float32 [131072, 2], P(('ep', 'tp')), may hold values from 0.1 to 1
- w_gate: bfloat16 [32, 2048, 512], P('ep', None, 'tp'), may hold values from -0.125 to 0.125
- w_up: bfloat16 [32, 2048, 512], P('ep', None, 'tp'), may hold values from -0.125 to 0.125
- w_down: bfloat16 [32, 2048, 512], P('ep', None, 'tp'), may hold values from -0.25 to 0.25
Outputs:
- layer_out: bfloat16 [131072, 2048], P(('ep', 'tp'))
Inputs may be any that keep to these rules, and one draw needn't show every extreme that they name: `expert_ids`: each token names two different experts of one group, group g being experts 4 * g to 4 * g + 3. Among the rows of one device (aligned blocks of 256 rows) no expert is named more than 32 times, and in every block some expert is named exactly 32 times; one expert is named 32 times in every block.
All inputs are finite; a program needn't handle non-finite values.
Results may differ from a plain program's by a relative error of at most 0.0071.
Values may be sent and summed in bfloat16 or wider, within the bound.
A program may use at most 64 MiB of HBM per device.

v0:
```python
import jax
import jax.numpy as jnp
from jax import lax
from jax.sharding import PartitionSpec as P


def gather_turned(arrays, axis, dims):
    turned = [jnp.moveaxis(a, dim, 0) for a, dim in zip(arrays, dims)]
    both = jnp.concatenate([t.reshape(len(t), -1) for t in turned], axis=1)
    result, at, outs = (lax.all_gather(both, axis, axis=0, tiled=True), 0, [])
    for t, dim in zip(turned, dims):
        slab = result[:, at : at + t[0].size].reshape(-1, *t.shape[1:])
        outs.append(jnp.moveaxis(slab, 0, dim))
        at += t[0].size
    return tuple(outs)


def rms_scale(values, gain):
    mean_sq = jnp.mean(values * values, axis=-1, keepdims=True)
    return values * lax.rsqrt(mean_sq + 1e-06) * gain


def expert_terms(rows, gate_part, up_part, down_part):
    gate = jnp.dot(rows, gate_part, preferred_element_type=jnp.float32)
    up = jnp.dot(rows, up_part, preferred_element_type=jnp.float32)
    hidden = (jax.nn.silu(gate) * up).astype(jnp.bfloat16)
    return lax.dot_general(
        hidden, down_part, (((1,), (1,)), ((), ())), preferred_element_type=jnp.float32
    )


def collect_expert(w_gate, w_up, w_down):
    return gather_turned((w_gate, w_up, w_down), "tp", (2, 2, 2))


def body(tokens, pre_gain, post_gain, expert_ids, route_weight, w_gate, w_up, w_down):
    count, width = tokens.shape
    top = expert_ids.shape[1]
    experts = lax.axis_size("ep") * w_gate.shape[0]
    capacity = 2 * top * count // experts
    normed = rms_scale(tokens.astype(jnp.float32), pre_gain).astype(jnp.bfloat16)
    flat = expert_ids.reshape(-1)
    onehot = (flat[:, None] == jnp.arange(experts, dtype=jnp.int32)[None, :]).astype(jnp.int32)
    rank = jnp.sum((jnp.cumsum(onehot, axis=0) - onehot) * onehot, axis=1)
    target = flat * capacity + rank
    source = jnp.full((experts * capacity,), count, jnp.int32)
    source = source.at[target].set(jnp.arange(count * top, dtype=jnp.int32) // top)
    padded = jnp.concatenate([normed, jnp.zeros((1, width), jnp.bfloat16)], axis=0)
    outgoing = padded[source].reshape(experts, capacity, width)
    arrived = lax.all_to_all(outgoing, "ep", split_axis=0, concat_axis=0, tiled=True)
    rows = arrived.reshape(experts * capacity, width)
    gate_all, up_all, down_all = collect_expert(w_gate, w_up, w_down)
    result = expert_terms(rows, gate_all[0], up_all[0], down_all[0])
    answer = result.astype(jnp.bfloat16).reshape(experts, capacity, width)
    returned = lax.all_to_all(answer, "ep", split_axis=0, concat_axis=0, tiled=True)
    per_route = returned.reshape(experts * capacity, width)[target].reshape(count, top, width)
    mixed = jnp.sum(per_route.astype(jnp.float32) * route_weight[:, :, None], axis=1)
    return rms_scale(mixed, post_gain).astype(jnp.bfloat16)


def solution(mesh):
    in_specs = (
        P(("ep", "tp"), None),
        P(),
        P(),
        P(("ep", "tp"), None),
        P(("ep", "tp"), None),
        P("ep", None, "tp"),
        P("ep", None, "tp"),
        P("ep", None, "tp"),
    )
    out_specs = P(("ep", "tp"), None)
    return jax.shard_map(body, mesh=mesh, in_specs=in_specs, out_specs=out_specs, check_vma=False)
```

profile of v0, /device:TPU:1, one launch (start us, length us, event | category | flops | bytes accessed | tf_op | source)
XLA Modules:
  0.0 272.3 jit_solution(11717123274236315875)
XLA Ops:
  6.5 0.0 copy-start
  6.5 0.0 copy-start.1
  6.5 0.0 all-gather.2.cloned.1.call-start
  6.5 1.9 pad_maximum_fusion
  8.4 0.0 all-gather.2.cloned.1.call-update
  8.5 0.8 copy.11
  9.3 0.1 eq.29
  9.4 0.1 eq.25
  9.6 1.2 reduce-window.6
  10.7 0.2 slice_reduce_fusion
  11.0 0.7 broadcast_multiply_fusion
  11.7 0.1 copy.10
  11.8 0.1 mul.79
  12.0 0.0 copy-done
  12.0 0.3 fusion
  12.3 0.0 copy-done.1
  12.3 0.3 fusion.2
  12.6 0.1 concatenate.6
  12.7 0.1 fusion.8
  12.8 2.4 scatter_custom_fusion
  15.3 6.1 %gather_fusion = bf16[1024,2048]{1,0:T(8,128)(2,1)} fusion(bf16[257,2048]{1,0:T(8,128)(2,1)S(1)} %concatenate.6, s32[1024]{0:T(1024)S(1)} %fusion.10), kind=kCustom, calls=%fused_computation | custom fusion | bytes 8392704 | tf_op jit(solution)/shard_map/gather | solution.py:49
  21.4 107.4 %all_to_all.10 = bf16[32,32,2048]{2,1,0:T(8,128)(2,1)} all-to-all(bf16[32,32,2048]{2,1,0:T(8,128)(2,1)} %bitcast.61), channel_id=1, replica_groups=mesh['ep'=32,'tp'=16] {'ep'}, dimensions={0} | all-to-all | bytes 8388608 | tf_op jit(solution)/shard_map/all_to_all | solution.py:50
  128.8 0.0 all-gather.2.cloned.1.call-done
  128.8 5.2 %fusion.4 = f32[1024,512]{1,0:T(8,128)S(1)} fusion(bf16[1024,2048]{1,0:T(8,128)(2,1)} %bitcast.63, bf16[512,6144]{1,0:T(8,128)(2,1)} %all-gather.2.cloned.1.call-done), kind=kOutput, calls=%fused_computation.14 | convolution fusion | flops 2147483648 | bytes 8388608 | tf_op jit(solution)/shard_map/dot_general | solution.py:24
  134.0 10.2 %convolution_convert_fusion = bf16[1024,2048]{1,0:T(8,128)(2,1)} fusion(bf16[512,6144]{1,0:T(8,128)(2,1)} %all-gather.2.cloned.1.call-done, f32[1024,512]{1,0:T(8,128)S(1)} %fusion.4, bf16[1024,2048]{1,0:T(8,128)(2,1)} %bitcast.64), kind=kOutput, calls=%fused_computation.4 | convolution fusion | flops 4300210176 | bytes 14680064 | tf_op jit(solution)/shard_map/dot_general | solution.py:27
  144.2 0.0 copy-start.3
  144.2 6.8 %all-to-all-start.1 = ((bf16[32,32,2048]{2,1,0:T(8,128)(2,1)}), bf16[32,32,2048]{2,1,0:T(8,128)(2,1)}, u32[]{:S(2)}, u32[]{:S(2)}) async-start(bf16[32,32,2048]{2,1,0:T(8,128)(2,1)} %bitcast.62), calls=%async_computation.1 | async-start | bytes 8388608 | tf_op jit(solution)/shard_map/all_to_all | solution.py:55
  151.1 0.0 copy-done.3
  151.1 0.1 copy.14
  151.2 92.3 %all-to-all-done.1 = bf16[32,32,2048]{2,1,0:T(8,128)(2,1)} async-done(((bf16[32,32,2048]{2,1,0:T(8,128)(2,1)}), bf16[32,32,2048]{2,1,0:T(8,128)(2,1)}, u32[]{:S(2)}, u32[]{:S(2)}) %all-to-all-start.1) | async-done | bytes 4194336 | tf_op jit(solution)/shard_map/all_to_all | solution.py:55
  243.5 7.1 %gather_fusion.1 = bf16[512,2048]{1,0:T(8,128)(2,1)S(1)} fusion(bf16[1024,2048]{1,0:T(8,128)(2,1)} %bitcast.21, s32[1024]{0:T(1024)S(1)} %pad_clamp_fusion), kind=kCustom, calls=%fused_computation.1 | custom fusion | bytes 4196352 | tf_op jit(solution)/shard_map/gather | solution.py:56
  250.7 4.0 %reshape.109 = f32[256,2,2048]{2,1,0:T(2,128)} reshape(bf16[512,2048]{1,0:T(8,128)(2,1)S(1)} %gather_fusion.1) | data formatting | bytes 6291456 | tf_op jit(solution)/shard_map/convert_element_type | solution.py:57
  254.7 8.9 %multiply_reduce_fusion = f32[256,2048]{1,0:T(8,128)S(1)} fusion(f32[256,2,2048]{2,1,0:T(2,128)} %reshape.109, f32[256,2]{1,0:T(8,128)S(1)} %copy.14), kind=kLoop, calls=%fused_computation.3 | loop fusion | flops 1572864 | bytes 6293504 | tf_op jit(solution)/shard_map/reduce_sum | solution.py:57
  263.6 0.0 copy-start.2
  263.6 0.2 multiply_reduce_fusion.1
  263.8 0.5 copy-done.2
  264.3 1.2 multiply_convert_fusion
  (9 shorter events, 0.1 us)
Async XLA Ops:
  6.5 5.5 %copy-start = (bf16[256,2048]{1,0:T(8,128)(2,1)S(1)}, bf16[256,2048]{1,0:T(8,128)(2,1)}, u32[]{:S(2)}) copy-start(bf16[256,2048]{1,0:T(8,128)(2,1)} %param.8) | copy-start | bytes 3145732
  6.5 5.8 %copy-start.1 = (f32[2048]{0:T(1024)S(1)}, f32[2048]{0:T(1024)}, u32[]{:S(2)}) copy-start(f32[2048]{0:T(1024)} %param.9) | copy-start | bytes 24580
  6.5 122.2 %all-gather.2.cloned.1.call-start = ((), (), s32[]{:S(2)}) async-start(), calls=%async_computation.2 | async-start | bytes 6684672 | tf_op jit(solution)/shard_map/all_gather | solution.py:10
  144.2 6.8 %copy-start.3 = (f32[256,2]{0,1:T(2,128)S(1)}, f32[256,2]{0,1:T(2,128)}, u32[]{:S(2)}) copy-start(f32[256,2]{0,1:T(2,128)} %param.12) | copy-start | bytes 6148
  144.2 99.3 %all-to-all-start.1 = ((bf16[32,32,2048]{2,1,0:T(8,128)(2,1)}), bf16[32,32,2048]{2,1,0:T(8,128)(2,1)}, u32[]{:S(2)}, u32[]{:S(2)}) async-start(bf16[32,32,2048]{2,1,0:T(8,128)(2,1)} %bitcast.62), calls=%async_computation.1 | async-start | bytes 8388608 | tf_op jit(solution)/shard_map/all_to_all | solution.py:55
  263.6 0.7 copy-start.2
Sparse Core Ops, SparseCore 0:
  9.5 54.4 all-gather.1
where the time goes:
time: 275 us; the launch traced here: 272 us
  blocking collectives  107 us (39%)
  waiting for transfers between devices  92.3 us (34%)
  local copies, waits for them, and re-layouts  21.9 us (8%)
  matrix products  15.4 us (6%)
  other arithmetic  14.8 us (5%)
  between operations  13.6 us (5%)
  starting transfers between devices  6.83 us (2%)
    all_to_all x1, blocking collectives, body(): lax.all_to_all(outgoing, 'ep', split_axis=0, concat_axis=0, tiled=True)  107 us
    all_to_all x1, waiting for transfers between devices, body(): lax.all_to_all(answer, 'ep', split_axis=0, concat_axis=0, tiled=True)  92.3 us
    dot_general x1, matrix products, expert_terms(): lax.dot_general(hidden, down_part, (((1,), (1,)), ((), ())), preferred_el...  10.2 us
    reduce_sum x1, other arithmetic, body(): jnp.sum(per_route.astype(jnp.float32) * route_weight[:, :, None], axis=1)  8.89 us
    gather x1, local copies, waits for them, and re-layouts, body(): returned.reshape(experts * capacity, width)[target]  7.13 us
    all_to_all x1, starting transfers between devices, body(): lax.all_to_all(answer, 'ep', split_axis=0, concat_axis=0, tiled=True)  6.82 us
    gather x1, local copies, waits for them, and re-layouts, body(): outgoing = padded[source].reshape(experts, capacity, width)  6.07 us
  transfers between devices with their start and end apart: 2, of which 1 were waited for; matrix products, arithmetic and copies ran while one was open for 5% of the time, Pallas kernels for 0%

commit v1 on v0

v1 whole, which is shorter than its diff:
```python
import jax
import jax.numpy as jnp
from jax import lax
from jax.experimental import pallas as pl
from jax.experimental.pallas import tpu as pltpu
from jax.sharding import PartitionSpec as P

MESH = pl.DeviceIdType.MESH
BF16 = jnp.bfloat16
F32 = jnp.float32
WIDTH = 2048
TOKENS = 256
PART = 32
FF = 512
ZS = 8
XS = 4
YS = 8
SLOT = 64
CAP = 32
COLS = 512
DELTA = (2, 6, 1, 7, 3, 5, 4, 0)
OWN = 7
STEP_X = (1, 3, 2)


def nt_dot(a, b):
    return lax.dot_general(a, b, (((1,), (1,)), ((), ())), preferred_element_type=F32)


def tn_dot(a, b):
    return lax.dot_general(a, b, (((0,), (0,)), ((), ())), preferred_element_type=F32)


def nn_dot(a, b):
    return jnp.dot(a, b, preferred_element_type=F32)


def iota(shape, dim):
    return lax.broadcasted_iota(jnp.int32, shape, dim)


def rms_scale(values, gain):
    mean_sq = jnp.mean(values * values, axis=-1, keepdims=True)
    return values * lax.rsqrt(mean_sq + 1e-06) * gain


def kernel(
    tok_ref, pre_ref, post_ref, ids_ref, rw_ref, wg_ref, wu_ref, wd_ref, out_ref,
    normed, onehot, zsend, msend, zrecv, mrecv, xsend, xrecv, wall, ores, xret, zback, zfin, mixed,
    zs_sem, zr_sem, ms_sem, mr_sem, xs_sem, xr_sem, os_sem, or_sem, bs_sem, br_sem,
    ws_sem, wr_sem, ds_sem, dr_sem,
):
    ep, tp = lax.axis_index("ep"), lax.axis_index("tp")
    z, x = ep // XS, ep % XS
    y, core = tp // 2, tp % 2

    def at_z(step):
        return (lax.rem(z + step, ZS) * XS + x, tp)

    def at_x(step):
        return (z * XS + lax.rem(x + step, XS), tp)

    def at_y(step):
        return (ep, lax.rem(y + step, YS) * 2 + core)

    other = (ep, y * 2 + (1 - core))

    def remote(src, dst, send, recv, device):
        return pltpu.make_async_remote_copy(
            src_ref=src, dst_ref=dst, send_sem=send, recv_sem=recv,
            device_id=device, device_id_type=MESH,
        )

    barrier = pltpu.get_barrier_semaphore()
    partners = [at_z(k) for k in range(1, ZS)] + [at_x(k) for k in range(1, XS)]
    partners += [at_y(1), at_y(YS - 1), other]
    for device in partners:
        pl.semaphore_signal(barrier, inc=1, device_id=device, device_id_type=MESH)

    for m, ref in enumerate((wg_ref, wu_ref, wd_ref)):
        wall[m, 0] = ref[...]
    for r in range(0, TOKENS, 32):
        rows = tok_ref[pl.ds(r, 32), :].astype(F32)
        normed[pl.ds(r, 32), :] = rms_scale(rows, pre_ref[...]).astype(BF16)
    ids0, ids1 = ids_ref[0:1, :], ids_ref[1:2, :]
    rw0, rw1 = rw_ref[0:1, :], rw_ref[1:2, :]
    before = (iota((TOKENS, TOKENS), 0) < iota((TOKENS, TOKENS), 1)).astype(F32).astype(BF16)
    row = iota((ZS * 8, 1), 0)
    place = row // 8
    delta = jnp.zeros_like(place)
    for p, d in enumerate(DELTA):
        delta = jnp.where(place == p, d, delta)
    home = lax.rem(z + delta, ZS)
    expert = jnp.where(row % 8 < XS, home * XS + row % 8, -1)
    first, second = ids0 == expert, ids1 == expert
    chosen = (first | second).astype(F32)
    rank = nn_dot(chosen.astype(BF16), before)
    rank1 = (rank + 1.0) * chosen
    weight = jnp.where(first, rw0, 0.0) + jnp.where(second, rw1, 0.0)
    w_hi = weight.astype(BF16).astype(F32)
    w_lo = weight - w_hi
    place8 = iota((ZS, 1), 0)
    delta8 = jnp.zeros_like(place8)
    for p, d in enumerate(DELTA):
        delta8 = jnp.where(place8 == p, d, delta8)
    in_group = (ids0 // XS == lax.rem(z + delta8, ZS)).astype(F32)
    slot_all = nn_dot(in_group.astype(BF16), before)
    spot = jnp.sum(
        in_group * (slot_all + (place8 * SLOT).astype(F32)), axis=0, keepdims=True
    ).astype(jnp.int32)
    for p in range(ZS):
        onehot[p] = (iota((SLOT, TOKENS), 0) + p * SLOT == spot).astype(F32).astype(BF16)

    pl.semaphore_wait(barrier, len(partners))

    def ring(step):
        if step < 4:
            ahead = (wall.at[:, step - 1], wall.at[:, step])
            back = (wall.at[:, (YS - step + 1) % YS], wall.at[:, YS - step])
        else:
            low, high = pl.ds(0, PART // 2), pl.ds(PART // 2, PART // 2)
            ahead = (wall.at[:, 3, low], wall.at[:, 4, low])
            back = (wall.at[:, 5, high], wall.at[:, 4, high])
        k = step - 1
        return [
            remote(*ahead, ws_sem.at[0, k], wr_sem.at[0, k], at_y(1)),
            remote(*back, ws_sem.at[1, k], wr_sem.at[1, k], at_y(YS - 1)),
        ]

    rings = {step: ring(step) for step in (1, 2, 3, 4)}
    dies = [
        remote(wall.at[:, m], wall.at[:, YS + m], ds_sem.at[m], dr_sem.at[m], other)
        for m in range(YS)
    ]

    def relay(step):
        for copy in rings[step]:
            copy.wait_recv()
        if step < 4:
            for copy in rings[step + 1]:
                copy.start()
        for m in (step, YS - step) if step < 4 else (4,):
            dies[m].start()

    for copy in rings[1]:
        copy.start()
    dies[0].start()

    z_out, m_out = {}, {}

    def send_plane(p):
        chosen_rows = onehot[p]
        meta = jnp.concatenate(
            [rank1[8 * p : 8 * p + 8], w_hi[8 * p : 8 * p + 8], w_lo[8 * p : 8 * p + 8],
             jnp.zeros((8, TOKENS), F32)], axis=0,
        ).astype(BF16)
        meta = nt_dot(meta, chosen_rows).astype(BF16)
        meta = jnp.concatenate([meta, jnp.zeros((32, 128 - SLOT), BF16)], axis=1)
        to_rows, to_meta = (zrecv, mrecv) if p == OWN else (zsend, msend)
        to_meta[p] = meta
        for c in range(0, WIDTH, COLS):
            part = nn_dot(chosen_rows, normed[:, c : c + COLS])
            to_rows[p, :, c : c + COLS] = part.astype(BF16)
        if p != OWN:
            m_out[p] = remote(msend.at[p], mrecv.at[p], ms_sem.at[p], mr_sem.at[p], at_z(DELTA[p]))
            z_out[p] = remote(zsend.at[p], zrecv.at[p], zs_sem.at[p], zr_sem.at[p], at_z(DELTA[p]))
            m_out[p].start()
            z_out[p].start()

    def selector(p):
        meta = mrecv[p].astype(F32)[:, :SLOT]
        want = (iota((CAP, SLOT), 0) + 1).astype(F32)
        return meta, [(meta[i : i + 1, :] == want).astype(F32) for i in range(XS)]

    x_out, o_out = {}, {}

    def send_experts(p):
        if p != OWN:
            m_out[p].wait_recv()
            z_out[p].wait_recv()
        pick = jnp.concatenate(selector(p)[1], axis=0).astype(BF16)
        for c in range(0, WIDTH, COLS):
            part = nn_dot(pick, zrecv[p, :, c : c + COLS]).astype(BF16)
            xsend[p, :, :, c : c + COLS] = part.reshape(XS, CAP, COLS)
        for j, step in enumerate(STEP_X):
            x_out[p, j] = remote(
                xsend.at[p, lax.rem(x + step, XS)], xrecv.at[p, j + 1],
                xs_sem.at[p, j], xr_sem.at[p, j], at_x(step),
            )
            x_out[p, j].start()
        xrecv[p, 0] = xsend[p, x]

    def experts(p):
        for q in (p, p + 1):
            for j in range(XS - 1):
                x_out[q, j].wait_recv()
        rows = xrecv[pl.ds(p, 2)].reshape(2 * XS * CAP, WIDTH)
        gate = nt_dot(rows, wall[0].reshape(FF, WIDTH))
        up = nt_dot(rows, wall[1].reshape(FF, WIDTH))
        hidden = (gate / (1.0 + jnp.exp(-gate)) * up).astype(BF16)
        for c in range(0, WIDTH, COLS):
            part = nn_dot(hidden, wall[2, :, :, c : c + COLS].reshape(FF, COLS)).astype(BF16)
            ores[pl.ds(p, 2), :, :, c : c + COLS] = part.reshape(2, XS, CAP, COLS)
        for q in (p, p + 1):
            for j, step in enumerate(STEP_X):
                o_out[q, j] = remote(
                    ores.at[q, j + 1], xret.at[q, x],
                    os_sem.at[q, j], or_sem.at[q, j], at_x(XS - step),
                )
                o_out[q, j].start()
            xret[q, x] = ores[q, 0]

    b_out = {}

    def combine(p):
        for j, step in enumerate(STEP_X):
            remote(
                ores.at[p, j + 1], xret.at[p, lax.rem(x + step, XS)],
                os_sem.at[p, j], or_sem.at[p, j], at_x(XS - step),
            ).wait_recv()
        meta, picks = selector(p)
        hi = jnp.concatenate(
            [pick * meta[8 + i : 9 + i, :] for i, pick in enumerate(picks)], axis=0
        ).astype(BF16)
        lo = jnp.concatenate(
            [pick * meta[16 + i : 17 + i, :] for i, pick in enumerate(picks)], axis=0
        ).astype(BF16)
        to_rows = zfin if p == OWN else zback
        for c in range(0, WIDTH, COLS):
            rows = xret[p, :, :, c : c + COLS].reshape(XS * CAP, COLS)
            to_rows[p, :, c : c + COLS] = (tn_dot(hi, rows) + tn_dot(lo, rows)).astype(BF16)
        if p != OWN:
            b_out[p] = remote(
                zback.at[p], zfin.at[p], bs_sem.at[p], br_sem.at[p], at_z(ZS - DELTA[p])
            )
            b_out[p].start()

    send_plane(2)
    send_plane(3)
    send_plane(OWN)
    send_experts(OWN)
    for p in (0, 1, 4, 5, 6):
        send_plane(p)
    send_experts(2)
    send_experts(3)
    relay(1)
    send_experts(0)
    send_experts(1)
    relay(2)
    relay(3)
    send_experts(4)
    send_experts(5)
    relay(4)
    for copy in dies:
        copy.wait_recv()
    experts(0)
    send_experts(6)
    experts(2)
    combine(0)
    combine(1)
    experts(4)
    combine(2)
    combine(3)
    experts(6)
    combine(4)
    combine(5)
    combine(6)
    combine(7)
    for p in range(ZS - 1):
        b_out[p].wait_recv()
    for c in range(0, WIDTH, COLS):
        rows = zfin[:, :, c : c + COLS].reshape(ZS * SLOT, COLS)
        mixed[:, c : c + COLS] = tn_dot(onehot[...].reshape(ZS * SLOT, TOKENS), rows)
    for r in range(0, TOKENS, 32):
        out_ref[pl.ds(r, 32), :] = rms_scale(mixed[pl.ds(r, 32), :], post_ref[...]).astype(BF16)
    for step in rings:
        for copy in rings[step]:
            copy.wait_send()
    for copies in (dies, m_out.values(), z_out.values(), x_out.values(), o_out.values(), b_out.values()):
        for copy in copies:
            copy.wait_send()


def body(tokens, pre_gain, post_gain, expert_ids, route_weight, w_gate, w_up, w_down):
    dma = pltpu.SemaphoreType.DMA
    vmem = pltpu.VMEM
    return pl.pallas_call(
        kernel,
        name="experts",
        out_shape=jax.ShapeDtypeStruct((TOKENS, WIDTH), BF16),
        in_specs=[pl.BlockSpec(memory_space=vmem)] * 8,
        out_specs=pl.BlockSpec(memory_space=vmem),
        scratch_shapes=[
            vmem((TOKENS, WIDTH), BF16),
            vmem((ZS, SLOT, TOKENS), BF16),
            vmem((ZS, SLOT, WIDTH), BF16),
            vmem((ZS, 32, 128), BF16),
            vmem((ZS, SLOT, WIDTH), BF16),
            vmem((ZS, 32, 128), BF16),
            vmem((ZS, XS, CAP, WIDTH), BF16),
            vmem((ZS, XS, CAP, WIDTH), BF16),
            vmem((3, 2 * YS, PART, WIDTH), BF16),
            vmem((ZS, XS, CAP, WIDTH), BF16),
            vmem((ZS, XS, CAP, WIDTH), BF16),
            vmem((ZS, SLOT, WIDTH), BF16),
            vmem((ZS, SLOT, WIDTH), BF16),
            vmem((TOKENS, WIDTH), F32),
            dma((ZS,)), dma((ZS,)), dma((ZS,)), dma((ZS,)),
            dma((ZS, XS - 1)), dma((ZS, XS - 1)), dma((ZS, XS - 1)), dma((ZS, XS - 1)),
            dma((ZS,)), dma((ZS,)),
            dma((2, 4)), dma((2, 4)), dma((YS,)), dma((YS,)),
        ],
        compiler_params=pltpu.CompilerParams(
            collective_id=0, has_side_effects=True, vmem_limit_bytes=60 << 20
        ),
    )(
        tokens, pre_gain[None], post_gain[None], expert_ids.T, route_weight.T,
        w_gate[0].T, w_up[0].T, w_down[0].T,
    )


def solution(mesh):
    in_specs = (
        P(("ep", "tp"), None),
        P(),
        P(),
        P(("ep", "tp"), None),
        P(("ep", "tp"), None),
        P("ep", None, "tp"),
        P("ep", None, "tp"),
        P("ep", None, "tp"),
    )
    out_specs = P(("ep", "tp"), None)
    return jax.shard_map(body, mesh=mesh, in_specs=in_specs, out_specs=out_specs, check_vma=False)
```

time: 275 us -> 139 us (0.51)
  the two profiles are of different devices: /device:TPU:1 before, /device:TPU:384 now
where the time goes in v1:
time: 139 us
  Pallas kernels  137 us (99%)
  local copies, waits for them, and re-layouts  2.3 us (2%)
    pallas_call x1, Pallas kernels, body(): pl.pallas_call(kernel, name='experts', out_shape=jax.ShapeDtypeStruct((TO...  137 us

profile of v1, /device:TPU:384, one launch (start us, length us, event | category | flops | bytes accessed | tf_op | source)
XLA Modules:
  0.0 139.1 jit_solution(8141014871641057992)
XLA Ops:
  0.0 136.8 %experts.1 = bf16[256,2048]{1,0:T(8,128)(2,1)} custom-call(bf16[256,2048]{1,0:T(8,128)(2,1)} %tok_ref.1, f32[1,2048]{1,0:T(1,128)} %bitcast.16, f32[1,2048]{1,0:T(1,128)} %bitcast.17, s32[2,256]{1,0:T(2,128)} %bitcast.18, f32[2,256]{1,0:T(2,128)} %bitcast.19, bf16[32,2048]{1,0:T(8,128)(2,1)} %bitcast.13, bf16[32,2048]{1,0:T(8,128)(2,1)} %bitcast.14, ...), custom_call_target="tpu_custom_call" | custom-call | tf_op jit(solution)/shard_map/experts/pallas_call | solution.py:287
  136.8 2.3 %copy.10 = bf16[256,2048]{1,0:T(8,128)(2,1)} copy(bf16[256,2048]{1,0:T(8,128)(2,1)} %experts.1) | data formatting | bytes 2097152

commit v2 on v1

v2 whole, which is shorter than its diff:
```python
import jax
import jax.numpy as jnp
from jax import lax
from jax.experimental import pallas as pl
from jax.experimental.pallas import tpu as pltpu
from jax.sharding import PartitionSpec as P

MESH = pl.DeviceIdType.MESH
BF16 = jnp.bfloat16
F32 = jnp.float32
WIDTH = 2048
TOKENS = 256
PART = 32
FF = 512
ZS = 8
XS = 4
YS = 8
SLOT = 64
CAP = 32
COLS = 512
DELTA = (1, 7, 2, 6, 3, 5, 0, 4)
STEP = (1, 7, 2, 6, 7, 1, 0, 0)
LOCAL = (6, 7)
STEP_X = (1, 3, 2)
HALF = PART // 2


def nt_dot(a, b):
    return lax.dot_general(a, b, (((1,), (1,)), ((), ())), preferred_element_type=F32)


def tn_dot(a, b):
    return lax.dot_general(a, b, (((0,), (0,)), ((), ())), preferred_element_type=F32)


def nn_dot(a, b):
    return jnp.dot(a, b, preferred_element_type=F32)


def iota(shape, dim):
    return lax.broadcasted_iota(jnp.int32, shape, dim)


def rms_scale(values, gain):
    mean_sq = jnp.mean(values * values, axis=-1, keepdims=True)
    return values * lax.rsqrt(mean_sq + 1e-06) * gain


def kernel(
    tok_hbm, pre_hbm, post_hbm, ids_hbm, rw_hbm, wg_hbm, wu_hbm, wd_hbm, out_ref,
    tok_ref, pre_ref, post_ref, ids_ref, rw_ref, in_sem, normed, onehot, zsend, msend, zrecv, mrecv, xsend, xrecv, near, far, ores, xret, zback, zfin, mixed,
    zs_sem, zr_sem, ms_sem, mr_sem, xs_sem, xr_sem, os_sem, or_sem, bs_sem, br_sem,
    ws_sem, wr_sem, ds_sem, dr_sem, fs_sem, fr_sem, gs_sem, gr_sem, hs_sem, hr_sem,
):
    ep, tp = lax.axis_index("ep"), lax.axis_index("tp")
    z, x = ep // XS, ep % XS
    y, core = tp // 2, tp % 2

    def at_z(step):
        return (lax.rem(z + step, ZS) * XS + x, tp)

    def at_x(step):
        return (z * XS + lax.rem(x + step, XS), tp)

    def at_y(step):
        return (ep, lax.rem(y + step, YS) * 2 + core)

    other = (ep, y * 2 + (1 - core))

    def remote(src, dst, send, recv, device):
        return pltpu.make_async_remote_copy(
            src_ref=src, dst_ref=dst, send_sem=send, recv_sem=recv,
            device_id=device, device_id_type=MESH,
        )

    loads = [
        pltpu.make_async_copy(src, dst, in_sem.at[k])
        for k, (src, dst) in enumerate((
            (tok_hbm, tok_ref), (pre_hbm, pre_ref), (ids_hbm, ids_ref), (rw_hbm, rw_ref),
            (wg_hbm, near.at[0, 0]), (wu_hbm, near.at[1, 0]), (wd_hbm, near.at[2, 0]),
            (post_hbm, post_ref),
        ))
    ]
    for copy in loads:
        copy.start()
    barrier = pltpu.get_barrier_semaphore()
    partners = [at_z(k) for k in (1, 2, 4, 6, 7)] + [at_x(k) for k in range(1, XS)]
    partners += [at_y(1), at_y(YS - 1), other]
    for device in partners:
        pl.semaphore_signal(barrier, inc=1, device_id=device, device_id_type=MESH)

    for copy in loads:
        copy.wait()
    for r in range(0, TOKENS, 32):
        rows = tok_ref[pl.ds(r, 32), :].astype(F32)
        normed[pl.ds(r, 32), :] = rms_scale(rows, pre_ref[...]).astype(BF16)
    ids0, ids1 = ids_ref[0:1, :], ids_ref[1:2, :]
    rw0, rw1 = rw_ref[0:1, :], rw_ref[1:2, :]
    before = (iota((TOKENS, TOKENS), 0) < iota((TOKENS, TOKENS), 1)).astype(F32).astype(BF16)

    def home_of(place):
        delta = jnp.zeros_like(place)
        for p, d in enumerate(DELTA):
            delta = jnp.where(place == p, d, delta)
        return lax.rem(z + delta, ZS)

    row = iota((ZS * 8, 1), 0)
    expert = jnp.where(row % 8 < XS, home_of(row // 8) * XS + row % 8, -1)
    first, second = ids0 == expert, ids1 == expert
    chosen = (first | second).astype(F32)
    rank1 = (nn_dot(chosen.astype(BF16), before) + 1.0) * chosen
    weight = jnp.where(first, rw0, 0.0) + jnp.where(second, rw1, 0.0)
    w_hi = weight.astype(BF16).astype(F32)
    w_lo = weight - w_hi
    place8 = iota((ZS, 1), 0)
    in_group = (ids0 // XS == home_of(place8)).astype(F32)
    slot = nn_dot(in_group.astype(BF16), before) + (place8 * SLOT).astype(F32)
    spot = jnp.sum(in_group * slot, axis=0, keepdims=True).astype(jnp.int32)
    for p in range(ZS):
        onehot[p] = (iota((SLOT, TOKENS), 0) + p * SLOT == spot).astype(F32).astype(BF16)

    pl.semaphore_wait(barrier, len(partners))

    def part(name, m, h):
        return near.at[:, m, pl.ds(h * HALF, HALF)] if name == "near" else far.at[h, m]

    def ring(name, h, step, send, recv):
        k = step - 1
        pairs = [
            (part(name, step - 1, h), part(name, step, h)),
            (part(name, (YS - step + 1) % YS, h), part(name, YS - step, h)),
        ]
        if step == 4 and name == "near":
            pairs[1 - h] = None
        elif step == 4:
            low, high = pl.ds(0, HALF), pl.ds(HALF, HALF)
            pairs = [
                (far.at[h, 3, low], far.at[h, 4, low]),
                (far.at[h, 5, high], far.at[h, 4, high]),
            ]
        return [
            remote(*pair, send.at[h, way, k], recv.at[h, way, k], at_y((1, YS - 1)[way]))
            for way, pair in enumerate(pairs) if pair is not None
        ]

    rings, dies = {}, {}
    for name, count, sems in (
        ("near", 2, (ws_sem, wr_sem, ds_sem, dr_sem)), ("far", 3, (fs_sem, fr_sem, gs_sem, gr_sem))
    ):
        for h in range(count):
            for step in (1, 2, 3, 4):
                rings[name, h, step] = ring(name, h, step, *sems[:2])
            for m in range(YS):
                dies[name, h, m] = remote(
                    part(name, m, h), part(name, YS + m, h), sems[2].at[h, m], sems[3].at[h, m], other
                )

    shards = [
        remote(near.at[h, 0], far.at[h, 0], hs_sem.at[h], hr_sem.at[h], at_z(4)) for h in range(3)
    ]

    def relay(name, h, step):
        if step == 0:
            if name == "far":
                shards[h].wait_recv()
        else:
            for copy in rings[name, h, step]:
                copy.wait_recv()
        if step < 4:
            for copy in rings[name, h, step + 1]:
                copy.start()
        for m in sorted({step, (YS - step) % YS}):
            dies[name, h, m].start()

    def whole(name):
        for key, copy in dies.items():
            if key[0] == name:
                copy.wait_recv()

    z_out, m_out = {}, {}

    def send_plane(p):
        chosen_rows = onehot[p]
        meta = jnp.concatenate(
            [rank1[8 * p : 8 * p + 8], w_hi[8 * p : 8 * p + 8], w_lo[8 * p : 8 * p + 8],
             jnp.zeros((8, TOKENS), F32)], axis=0,
        ).astype(BF16)
        meta = nt_dot(meta, chosen_rows).astype(BF16)
        meta = jnp.concatenate([meta, jnp.zeros((32, 128 - SLOT), BF16)], axis=1)
        to_rows, to_meta = (zrecv, mrecv) if p in LOCAL else (zsend, msend)
        to_meta[p] = meta
        for c in range(0, WIDTH, COLS):
            block = nn_dot(chosen_rows, normed[:, c : c + COLS])
            to_rows[p, :, c : c + COLS] = block.astype(BF16)
        if p not in LOCAL:
            m_out[p] = remote(msend.at[p], mrecv.at[p], ms_sem.at[p], mr_sem.at[p], at_z(STEP[p]))
            z_out[p] = remote(zsend.at[p], zrecv.at[p], zs_sem.at[p], zr_sem.at[p], at_z(STEP[p]))
            m_out[p].start()
            z_out[p].start()

    def selector(p):
        meta = mrecv[p].astype(F32)[:, :SLOT]
        want = (iota((CAP, SLOT), 0) + 1).astype(F32)
        return meta, [(meta[i : i + 1, :] == want).astype(F32) for i in range(XS)]

    x_out, o_out = {}, {}

    def send_experts(p):
        if p not in LOCAL:
            m_out[p].wait_recv()
            z_out[p].wait_recv()
        pick = jnp.concatenate(selector(p)[1], axis=0).astype(BF16)
        for c in range(0, WIDTH, COLS):
            block = nn_dot(pick, zrecv[p, :, c : c + COLS]).astype(BF16)
            xsend[p, :, :, c : c + COLS] = block.reshape(XS, CAP, COLS)
        for j, step in enumerate(STEP_X):
            x_out[p, j] = remote(
                xsend.at[p, lax.rem(x + step, XS)], xrecv.at[p, j + 1],
                xs_sem.at[p, j], xr_sem.at[p, j], at_x(step),
            )
            x_out[p, j].start()
        xrecv[p, 0] = xsend[p, x]

    def experts(p, count, weights):
        for q in range(p, p + count):
            for j in range(XS - 1):
                x_out[q, j].wait_recv()
        rows = xrecv[pl.ds(p, count)].reshape(count * XS * CAP, WIDTH)
        gate = nt_dot(rows, weights[0].reshape(FF, WIDTH))
        up = nt_dot(rows, weights[1].reshape(FF, WIDTH))
        hidden = (gate / (1.0 + jnp.exp(-gate)) * up).astype(BF16)
        for c in range(0, WIDTH, COLS):
            block = nn_dot(hidden, weights[2, :, :, c : c + COLS].reshape(FF, COLS)).astype(BF16)
            ores[pl.ds(p, count), :, :, c : c + COLS] = block.reshape(count, XS, CAP, COLS)
        for q in range(p, p + count):
            for j, step in enumerate(STEP_X):
                o_out[q, j] = remote(
                    ores.at[q, j + 1], xret.at[q, x],
                    os_sem.at[q, j], or_sem.at[q, j], at_x(XS - step),
                )
                o_out[q, j].start()
            xret[q, x] = ores[q, 0]

    b_out = {}

    def combine(p):
        for j, step in enumerate(STEP_X):
            remote(
                ores.at[p, j + 1], xret.at[p, lax.rem(x + step, XS)],
                os_sem.at[p, j], or_sem.at[p, j], at_x(XS - step),
            ).wait_recv()
        meta, picks = selector(p)
        hi = jnp.concatenate(
            [pick * meta[8 + i : 9 + i, :] for i, pick in enumerate(picks)], axis=0
        ).astype(BF16)
        lo = jnp.concatenate(
            [pick * meta[16 + i : 17 + i, :] for i, pick in enumerate(picks)], axis=0
        ).astype(BF16)
        to_rows = zfin if p in LOCAL else zback
        for c in range(0, WIDTH, COLS):
            rows = xret[p, :, :, c : c + COLS].reshape(XS * CAP, COLS)
            to_rows[p, :, c : c + COLS] = (tn_dot(hi, rows) + tn_dot(lo, rows)).astype(BF16)
        if p not in LOCAL:
            b_out[p] = remote(
                zback.at[p], zfin.at[p], bs_sem.at[p], br_sem.at[p], at_z(ZS - STEP[p])
            )
            b_out[p].start()

    relay("near", 0, 0)
    relay("near", 1, 0)
    send_plane(6)
    send_experts(6)
    send_plane(0)
    send_plane(1)
    send_plane(7)
    send_experts(7)
    send_plane(4)
    send_plane(5)
    shards[0].start()
    send_plane(2)
    send_plane(3)
    relay("near", 0, 1)
    send_experts(0)
    send_experts(1)
    relay("near", 1, 1)
    relay("near", 0, 2)
    relay("near", 1, 2)
    send_experts(4)
    send_experts(5)
    relay("near", 0, 3)
    relay("near", 1, 3)
    relay("far", 0, 0)
    relay("near", 0, 4)
    relay("near", 1, 4)
    send_experts(2)
    send_experts(3)
    shards[1].start()
    shards[2].start()
    relay("far", 0, 1)
    relay("far", 0, 2)
    whole("near")
    experts(0, 2, near)
    relay("far", 1, 0)
    relay("far", 0, 3)
    relay("far", 1, 1)
    relay("far", 2, 0)
    experts(2, 2, near)
    relay("far", 0, 4)
    relay("far", 1, 2)
    relay("far", 2, 1)
    experts(6, 1, near)
    relay("far", 1, 3)
    relay("far", 2, 2)
    combine(0)
    combine(1)
    relay("far", 1, 4)
    relay("far", 2, 3)
    combine(2)
    relay("far", 2, 4)
    whole("far")
    experts(4, 2, far)
    combine(3)
    experts(7, 1, far)
    combine(6)
    combine(4)
    combine(5)
    combine(7)
    for p in range(ZS):
        if p not in LOCAL:
            b_out[p].wait_recv()
    for c in range(0, WIDTH, COLS):
        rows = zfin[:, :, c : c + COLS].reshape(ZS * SLOT, COLS)
        mixed[:, c : c + COLS] = tn_dot(onehot[...].reshape(ZS * SLOT, TOKENS), rows)
    for r in range(0, TOKENS, 32):
        out_ref[pl.ds(r, 32), :] = rms_scale(mixed[pl.ds(r, 32), :], post_ref[...]).astype(BF16)
    for copies in [*rings.values(), dies.values(), shards]:
        for copy in copies:
            copy.wait_send()
    for copies in (m_out, z_out, x_out, o_out, b_out):
        for copy in copies.values():
            copy.wait_send()


def body(tokens, pre_gain, post_gain, expert_ids, route_weight, w_gate, w_up, w_down):
    dma = pltpu.SemaphoreType.DMA
    vmem = pltpu.VMEM
    return pl.pallas_call(
        kernel,
        name="experts",
        out_shape=jax.ShapeDtypeStruct((TOKENS, WIDTH), BF16),
        in_specs=[pl.BlockSpec(memory_space=pltpu.HBM)] * 8,
        out_specs=pl.BlockSpec(memory_space=vmem),
        scratch_shapes=[
            vmem((TOKENS, WIDTH), BF16),
            vmem((1, WIDTH), F32),
            vmem((1, WIDTH), F32),
            vmem((2, TOKENS), jnp.int32),
            vmem((2, TOKENS), F32),
            dma((8,)),
            vmem((TOKENS, WIDTH), BF16),
            vmem((ZS, SLOT, TOKENS), BF16),
            vmem((ZS, SLOT, WIDTH), BF16),
            vmem((ZS, 32, 128), BF16),
            vmem((ZS, SLOT, WIDTH), BF16),
            vmem((ZS, 32, 128), BF16),
            vmem((ZS, XS, CAP, WIDTH), BF16),
            vmem((ZS, XS, CAP, WIDTH), BF16),
            vmem((3, 2 * YS, PART, WIDTH), BF16),
            vmem((3, 2 * YS, PART, WIDTH), BF16),
            vmem((ZS, XS, CAP, WIDTH), BF16),
            vmem((ZS, XS, CAP, WIDTH), BF16),
            vmem((ZS, SLOT, WIDTH), BF16),
            vmem((ZS, SLOT, WIDTH), BF16),
            vmem((TOKENS, WIDTH), F32),
            dma((ZS,)), dma((ZS,)), dma((ZS,)), dma((ZS,)),
            dma((ZS, XS - 1)), dma((ZS, XS - 1)), dma((ZS, XS - 1)), dma((ZS, XS - 1)),
            dma((ZS,)), dma((ZS,)),
            dma((2, 2, 4)), dma((2, 2, 4)), dma((2, YS)), dma((2, YS)),
            dma((3, 2, 4)), dma((3, 2, 4)), dma((3, YS)), dma((3, YS)), dma((3,)), dma((3,)),
        ],
        compiler_params=pltpu.CompilerParams(
            collective_id=0, has_side_effects=True, vmem_limit_bytes=52 << 20
        ),
    )(*[
        pltpu.with_memory_space_constraint(a, pltpu.HBM)
        for a in (
            tokens, pre_gain[None], post_gain[None], expert_ids.T, route_weight.T,
            w_gate[0].T, w_up[0].T, w_down[0].T,
        )
    ])


def solution(mesh):
    in_specs = (
        P(("ep", "tp"), None),
        P(),
        P(),
        P(("ep", "tp"), None),
        P(("ep", "tp"), None),
        P("ep", None, "tp"),
        P("ep", None, "tp"),
        P("ep", None, "tp"),
    )
    out_specs = P(("ep", "tp"), None)
    return jax.shard_map(body, mesh=mesh, in_specs=in_specs, out_specs=out_specs, check_vma=False)
```

time: 139 us -> 117 us (0.84)
  the two profiles are of different devices: /device:TPU:384 before, /device:TPU:1 now
where the time goes in v2:
time: 117 us; the launch traced here: 116 us
  Pallas kernels  115 us (98%)
    pallas_call x1, Pallas kernels, body(): pl.pallas_call(kernel, name='experts', out_shape=jax.ShapeDtypeStruct((TO...  115 us

profile of v2, /device:TPU:1, one launch (start us, length us, event | category | flops | bytes accessed | tf_op | source)
XLA Modules:
  0.0 116.4 jit_solution(866485441848953697)
XLA Ops:
  0.0 115.4 %experts.1 = bf16[256,2048]{1,0:T(8,128)(2,1)S(1)} custom-call(bf16[256,2048]{1,0:T(8,128)(2,1)} %tok_hbm.1, f32[1,2048]{1,0:T(1,128)} %bitcast.16, f32[1,2048]{1,0:T(1,128)} %bitcast.17, s32[2,256]{1,0:T(2,128)} %bitcast.18, f32[2,256]{1,0:T(2,128)} %bitcast.19, bf16[32,2048]{1,0:T(8,128)(2,1)} %bitcast.13, bf16[32,2048]{1,0:T(8,128)(2,1)} %bitcast.14, ...), custom_call_target="tpu_custom_call" | custom-call | tf_op jit(solution)/shard_map/experts/pallas_call | solution.py:347
  115.4 1.0 copy.10

commit v3 on v2

--- a/solution.py
+++ b/solution.py
@@ -121,8 +121,12 @@
 
     pl.semaphore_wait(barrier, len(partners))
 
+    low, high = pl.ds(0, HALF), pl.ds(HALF, HALF)
+
     def part(name, m, h):
-        return near.at[:, m, pl.ds(h * HALF, HALF)] if name == "near" else far.at[h, m]
+        if name == "near":
+            return near.at[:, m, (low, high)[h]]
+        return (far.at[0, m], far.at[1, m, low], far.at[1, m, high], far.at[2, m])[h]
 
     def ring(name, h, step, send, recv):
         k = step - 1
@@ -132,12 +136,11 @@
         ]
         if step == 4 and name == "near":
             pairs[1 - h] = None
+        elif step == 4 and h in (1, 2):
+            pairs[2 - h] = None
         elif step == 4:
-            low, high = pl.ds(0, HALF), pl.ds(HALF, HALF)
-            pairs = [
-                (far.at[h, 3, low], far.at[h, 4, low]),
-                (far.at[h, 5, high], far.at[h, 4, high]),
-            ]
+            w = (0, 1, 1, 2)[h]
+            pairs = [(far.at[w, 3, low], far.at[w, 4, low]), (far.at[w, 5, high], far.at[w, 4, high])]
         return [
             remote(*pair, send.at[h, way, k], recv.at[h, way, k], at_y((1, YS - 1)[way]))
             for way, pair in enumerate(pairs) if pair is not None
@@ -145,7 +148,7 @@
 
     rings, dies = {}, {}
     for name, count, sems in (
-        ("near", 2, (ws_sem, wr_sem, ds_sem, dr_sem)), ("far", 3, (fs_sem, fr_sem, gs_sem, gr_sem))
+        ("near", 2, (ws_sem, wr_sem, ds_sem, dr_sem)), ("far", 4, (fs_sem, fr_sem, gs_sem, gr_sem))
     ):
         for h in range(count):
             for step in (1, 2, 3, 4):
@@ -155,22 +158,24 @@
                     part(name, m, h), part(name, YS + m, h), sems[2].at[h, m], sems[3].at[h, m], other
                 )
 
+    own = (near.at[0, 0], near.at[1, 0, low], near.at[1, 0, high], near.at[2, 0])
     shards = [
-        remote(near.at[h, 0], far.at[h, 0], hs_sem.at[h], hr_sem.at[h], at_z(4)) for h in range(3)
+        remote(own[h], part("far", 0, h), hs_sem.at[h], hr_sem.at[h], at_z(4)) for h in range(4)
     ]
 
-    def relay(name, h, step):
-        if step == 0:
-            if name == "far":
+    def relay(name, step, *chains):
+        for h in chains:
+            if step > 0:
+                for copy in rings[name, h, step]:
+                    copy.wait_recv()
+            elif name == "far":
                 shards[h].wait_recv()
-        else:
-            for copy in rings[name, h, step]:
-                copy.wait_recv()
-        if step < 4:
-            for copy in rings[name, h, step + 1]:
-                copy.start()
-        for m in sorted({step, (YS - step) % YS}):
-            dies[name, h, m].start()
+            if step < 4:
+                for copy in rings[name, h, step + 1]:
+                    copy.start()
+        for h in chains:
+            for m in sorted({step, (YS - step) % YS}):
+                dies[name, h, m].start()
 
     def whole(name):
         for key, copy in dies.items():
@@ -266,8 +271,17 @@
             )
             b_out[p].start()
 
-    relay("near", 0, 0)
-    relay("near", 1, 0)
+    def unsort(first, count, more):
+        for p in range(first, first + count):
+            if p not in LOCAL:
+                b_out[p].wait_recv()
+        picks = onehot[pl.ds(first, count)].reshape(count * SLOT, TOKENS)
+        for c in range(0, WIDTH, COLS):
+            rows = zfin[pl.ds(first, count), :, c : c + COLS].reshape(count * SLOT, COLS)
+            block = tn_dot(picks, rows)
+            mixed[:, c : c + COLS] = mixed[:, c : c + COLS] + block if more else block
+
+    relay("near", 0, 0, 1)
     send_plane(6)
     send_experts(6)
     send_plane(0)
@@ -277,46 +291,42 @@
     send_plane(4)
     send_plane(5)
     shards[0].start()
+    shards[1].start()
     send_plane(2)
     send_plane(3)
-    relay("near", 0, 1)
+    relay("near", 1, 0)
     send_experts(0)
     send_experts(1)
     relay("near", 1, 1)
-    relay("near", 0, 2)
-    relay("near", 1, 2)
+    relay("near", 2, 0)
+    relay("near", 2, 1)
     send_experts(4)
     send_experts(5)
-    relay("near", 0, 3)
-    relay("near", 1, 3)
-    relay("far", 0, 0)
-    relay("near", 0, 4)
-    relay("near", 1, 4)
+    relay("near", 3, 0)
+    relay("near", 3, 1)
+    relay("far", 0, 0, 1)
+    relay("near", 4, 0)
+    relay("near", 4, 1)
     send_experts(2)
     send_experts(3)
-    shards[1].start()
     shards[2].start()
-    relay("far", 0, 1)
-    relay("far", 0, 2)
+    shards[3].start()
+    relay("far", 1, 0, 1)
+    relay("far", 2, 0, 1)
     whole("near")
     experts(0, 2, near)
-    relay("far", 1, 0)
-    relay("far", 0, 3)
-    relay("far", 1, 1)
-    relay("far", 2, 0)
+    relay("far", 0, 2, 3)
+    relay("far", 3, 0, 1)
     experts(2, 2, near)
-    relay("far", 0, 4)
-    relay("far", 1, 2)
-    relay("far", 2, 1)
+    relay("far", 1, 2, 3)
+    relay("far", 4, 0, 1)
     experts(6, 1, near)
-    relay("far", 1, 3)
-    relay("far", 2, 2)
+    relay("far", 2, 2, 3)
     combine(0)
     combine(1)
-    relay("far", 1, 4)
-    relay("far", 2, 3)
+    relay("far", 3, 2, 3)
     combine(2)
-    relay("far", 2, 4)
+    relay("far", 4, 2, 3)
     whole("far")
     experts(4, 2, far)
     combine(3)
@@ -324,13 +334,9 @@
     combine(6)
     combine(4)
     combine(5)
+    unsort(0, 4, False)
     combine(7)
-    for p in range(ZS):
-        if p not in LOCAL:
-            b_out[p].wait_recv()
-    for c in range(0, WIDTH, COLS):
-        rows = zfin[:, :, c : c + COLS].reshape(ZS * SLOT, COLS)
-        mixed[:, c : c + COLS] = tn_dot(onehot[...].reshape(ZS * SLOT, TOKENS), rows)
+    unsort(4, 4, True)
     for r in range(0, TOKENS, 32):
         out_ref[pl.ds(r, 32), :] = rms_scale(mixed[pl.ds(r, 32), :], post_ref[...]).astype(BF16)
     for copies in [*rings.values(), dies.values(), shards]:
@@ -376,7 +382,7 @@
             dma((ZS, XS - 1)), dma((ZS, XS - 1)), dma((ZS, XS - 1)), dma((ZS, XS - 1)),
             dma((ZS,)), dma((ZS,)),
             dma((2, 2, 4)), dma((2, 2, 4)), dma((2, YS)), dma((2, YS)),
-            dma((3, 2, 4)), dma((3, 2, 4)), dma((3, YS)), dma((3, YS)), dma((3,)), dma((3,)),
+            dma((4, 2, 4)), dma((4, 2, 4)), dma((4, YS)), dma((4, YS)), dma((4,)), dma((4,)),
         ],
         compiler_params=pltpu.CompilerParams(
             collective_id=0, has_side_effects=True, vmem_limit_bytes=52 << 20

time: 117 us -> 114 us (0.974)
  Pallas kernels: 115 us -> 113 us
    pallas_call x1, Pallas kernels: 115 us -> 113 us  [body(): pl.pallas_call(kernel, name='experts', out_shape=jax.ShapeDtypeStruct((TO...]
where the time goes in v3:
time: 114 us
  Pallas kernels  113 us (99%)
    pallas_call x1, Pallas kernels, body(): pl.pallas_call(kernel, name='experts', out_shape=jax.ShapeDtypeStruct((TO...  113 us

profile of v3, /device:TPU:1, one launch (start us, length us, event | category | flops | bytes accessed | tf_op | source)
XLA Modules:
  0.0 113.6 jit_solution(17344959332036485859)
XLA Ops:
  0.0 112.7 %experts.1 = bf16[256,2048]{1,0:T(8,128)(2,1)S(1)} custom-call(bf16[256,2048]{1,0:T(8,128)(2,1)} %tok_hbm.1, f32[1,2048]{1,0:T(1,128)} %bitcast.16, f32[1,2048]{1,0:T(1,128)} %bitcast.17, s32[2,256]{1,0:T(2,128)} %bitcast.18, f32[2,256]{1,0:T(2,128)} %bitcast.19, bf16[32,2048]{1,0:T(8,128)(2,1)} %bitcast.13, bf16[32,2048]{1,0:T(8,128)(2,1)} %bitcast.14, ...), custom_call_target="tpu_custom_call" | custom-call | tf_op jit(solution)/shard_map/experts/pallas_call | solution.py:353
  112.7 1.0 copy.10

commit v4 on v3

--- a/solution.py
+++ b/solution.py
@@ -23,6 +23,7 @@
 LOCAL = (6, 7)
 STEP_X = (1, 3, 2)
 HALF = PART // 2
+BLOCK = 64
 
 
 def nt_dot(a, b):
@@ -48,7 +49,7 @@
 
 def kernel(
     tok_hbm, pre_hbm, post_hbm, ids_hbm, rw_hbm, wg_hbm, wu_hbm, wd_hbm, out_ref,
-    tok_ref, pre_ref, post_ref, ids_ref, rw_ref, in_sem, normed, onehot, zsend, msend, zrecv, mrecv, xsend, xrecv, near, far, ores, xret, zback, zfin, mixed,
+    tok_ref, pre_ref, post_ref, ids_ref, rw_ref, in_sem, normed, onehot, zsend, msend, zrecv, mrecv, xsend, xrecv, near, far, ores, xret, zback, zfin, mixed, hid,
     zs_sem, zr_sem, ms_sem, mr_sem, xs_sem, xr_sem, os_sem, or_sem, bs_sem, br_sem,
     ws_sem, wr_sem, ds_sem, dr_sem, fs_sem, fr_sem, gs_sem, gr_sem, hs_sem, hr_sem,
 ):
@@ -73,10 +74,12 @@
             device_id=device, device_id_type=MESH,
         )
 
+    blocks = [pl.ds(r, BLOCK) for r in range(0, TOKENS, BLOCK)]
     loads = [
         pltpu.make_async_copy(src, dst, in_sem.at[k])
         for k, (src, dst) in enumerate((
-            (tok_hbm, tok_ref), (pre_hbm, pre_ref), (ids_hbm, ids_ref), (rw_hbm, rw_ref),
+            (ids_hbm, ids_ref), (rw_hbm, rw_ref), (pre_hbm, pre_ref),
+            *[(tok_hbm.at[b], tok_ref.at[b]) for b in blocks],
             (wg_hbm, near.at[0, 0]), (wu_hbm, near.at[1, 0]), (wd_hbm, near.at[2, 0]),
             (post_hbm, post_ref),
         ))
@@ -89,11 +92,8 @@
     for device in partners:
         pl.semaphore_signal(barrier, inc=1, device_id=device, device_id_type=MESH)
 
-    for copy in loads:
+    for copy in loads[:3]:
         copy.wait()
-    for r in range(0, TOKENS, 32):
-        rows = tok_ref[pl.ds(r, 32), :].astype(F32)
-        normed[pl.ds(r, 32), :] = rms_scale(rows, pre_ref[...]).astype(BF16)
     ids0, ids1 = ids_ref[0:1, :], ids_ref[1:2, :]
     rw0, rw1 = rw_ref[0:1, :], rw_ref[1:2, :]
     before = (iota((TOKENS, TOKENS), 0) < iota((TOKENS, TOKENS), 1)).astype(F32).astype(BF16)
@@ -118,6 +118,14 @@
     spot = jnp.sum(in_group * slot, axis=0, keepdims=True).astype(jnp.int32)
     for p in range(ZS):
         onehot[p] = (iota((SLOT, TOKENS), 0) + p * SLOT == spot).astype(F32).astype(BF16)
+
+    for k, block in enumerate(blocks):
+        loads[3 + k].wait()
+        for r in range(0, BLOCK, 32):
+            rows = pl.ds(k * BLOCK + r, 32)
+            normed[rows, :] = rms_scale(tok_ref[rows, :].astype(F32), pre_ref[...]).astype(BF16)
+    for copy in loads[3 + len(blocks) :]:
+        copy.wait()
 
     pl.semaphore_wait(barrier, len(partners))
 
@@ -226,14 +234,24 @@
             x_out[p, j].start()
         xrecv[p, 0] = xsend[p, x]
 
-    def experts(p, count, weights):
-        for q in range(p, p + count):
-            for j in range(XS - 1):
-                x_out[q, j].wait_recv()
+    def units(p, count, weights, half):
+        if half == 0:
+            for q in range(p, p + count):
+                for j in range(XS - 1):
+                    x_out[q, j].wait_recv()
         rows = xrecv[pl.ds(p, count)].reshape(count * XS * CAP, WIDTH)
-        gate = nt_dot(rows, weights[0].reshape(FF, WIDTH))
-        up = nt_dot(rows, weights[1].reshape(FF, WIDTH))
-        hidden = (gate / (1.0 + jnp.exp(-gate)) * up).astype(BF16)
+        own_half = pl.ds(half * YS, YS)
+        gate = nt_dot(rows, weights[0, own_half].reshape(FF // 2, WIDTH))
+        up = nt_dot(rows, weights[1, own_half].reshape(FF // 2, WIDTH))
+        part_hidden = (gate / (1.0 + jnp.exp(-gate)) * up).astype(BF16)
+        at = half * (FF // 2)
+        hid[pl.ds(p, count), :, at : at + FF // 2] = part_hidden.reshape(count, XS * CAP, FF // 2)
+
+    def experts(p, count, weights, started=False):
+        if not started:
+            units(p, count, weights, 0)
+        units(p, count, weights, 1)
+        hidden = hid[pl.ds(p, count)].reshape(count * XS * CAP, FF)
         for c in range(0, WIDTH, COLS):
             block = nn_dot(hidden, weights[2, :, :, c : c + COLS].reshape(FF, COLS)).astype(BF16)
             ores[pl.ds(p, count), :, :, c : c + COLS] = block.reshape(count, XS, CAP, COLS)
@@ -327,8 +345,9 @@
     relay("far", 3, 2, 3)
     combine(2)
     relay("far", 4, 2, 3)
+    units(4, 2, far, 0)
     whole("far")
-    experts(4, 2, far)
+    experts(4, 2, far, True)
     combine(3)
     experts(7, 1, far)
     combine(6)
@@ -362,7 +381,7 @@
             vmem((1, WIDTH), F32),
             vmem((2, TOKENS), jnp.int32),
             vmem((2, TOKENS), F32),
-            dma((8,)),
+            dma((7 + TOKENS // BLOCK,)),
             vmem((TOKENS, WIDTH), BF16),
             vmem((ZS, SLOT, TOKENS), BF16),
             vmem((ZS, SLOT, WIDTH), BF16),
@@ -378,6 +397,7 @@
             vmem((ZS, SLOT, WIDTH), BF16),
             vmem((ZS, SLOT, WIDTH), BF16),
             vmem((TOKENS, WIDTH), F32),
+            vmem((ZS, XS * CAP, FF), BF16),
             dma((ZS,)), dma((ZS,)), dma((ZS,)), dma((ZS,)),
             dma((ZS, XS - 1)), dma((ZS, XS - 1)), dma((ZS, XS - 1)), dma((ZS, XS - 1)),
             dma((ZS,)), dma((ZS,)),

time: 114 us -> 113 us (level)
  Pallas kernels: 113 us -> 111 us
    pallas_call x1, Pallas kernels: 113 us -> 111 us  [body(): pl.pallas_call(kernel, name='experts', out_shape=jax.ShapeDtypeStruct((TO...]
where the time goes in v4:
time: 113 us; the launch traced here: 112 us
  Pallas kernels  111 us (98%)
    pallas_call x1, Pallas kernels, body(): pl.pallas_call(kernel, name='experts', out_shape=jax.ShapeDtypeStruct((TO...  111 us

profile of v4, /device:TPU:1, one launch (start us, length us, event | category | flops | bytes accessed | tf_op | source)
XLA Modules:
  0.0 112.0 jit_solution(14964344486874297691)
XLA Ops:
  0.0 111.0 %experts.1 = bf16[256,2048]{1,0:T(8,128)(2,1)S(1)} custom-call(bf16[256,2048]{1,0:T(8,128)(2,1)} %tok_hbm.1, f32[1,2048]{1,0:T(1,128)} %bitcast.16, f32[1,2048]{1,0:T(1,128)} %bitcast.17, s32[2,256]{1,0:T(2,128)} %bitcast.18, f32[2,256]{1,0:T(2,128)} %bitcast.19, bf16[32,2048]{1,0:T(8,128)(2,1)} %bitcast.13, bf16[32,2048]{1,0:T(8,128)(2,1)} %bitcast.14, ...), custom_call_target="tpu_custom_call" | custom-call | tf_op jit(solution)/shard_map/experts/pallas_call | solution.py:372
  111.1 1.0 copy.10
